TPU v7x, 512 devices: a whole 4x8x8 slice. The times are simulated.
512 devices in a mesh: sp: 32 (over z, x), tp: 16 (over y, core).
Axes of the slice: x: 4, y: 8, z: 8, core: 2. Of those that a mesh axis runs over, the one named last changes fastest.
Arguments:
- stream_in: bfloat16 [8192, 2048], P(('sp', 'tp')), may hold values from -6 to 6
- pre_gate: bfloat16 [8192, 1024], P('sp', 'tp'), may hold values from -6 to 6
- value_in: bfloat16 [8192, 1024], P('sp', 'tp'), may hold values from -6 to 6
- post_gate: bfloat16 [8192, 1024], P('sp', 'tp'), may hold values from -6 to 6
- conv_taps: bfloat16 [3, 1024], P(None, 'tp'), may hold values from -3 to 3
- out_weight: bfloat16 [1024, 2048], P('tp'), may hold values from -0.1875 to 0.1875
- route_ids: int32 [8192, 4], P('sp'), may hold values from 0 to 31, all different within a row; in each aligned block of 16 rows (0 to 15, 16 to 31, ...) at most 4 rows name the same one
- route_weight: float32 [8192, 4], P('sp'), may hold values from 0.1 to 1
- ffn_gain: bfloat16 [2048], replicated, may hold values from 0.099609375 to 1.8984375
- post_gain: bfloat16 [2048], replicated, may hold values from 0.099609375 to 1.8984375
- gate_proj: bfloat16 [32, 2048, 2048], P('sp', None, 'tp'), may hold values from -0.39648438 to 0.39648438
- up_proj: bfloat16 [32, 2048, 2048], P('sp', None, 'tp'), may hold values from -0.39648438 to 0.39648438
- down_proj: bfloat16 [32, 2048, 2048], P('sp', None, 'tp'), may hold values from -0.125 to 0.125
Outputs:
- layer_out: bfloat16 [8192, 2048], P(('sp', 'tp'))
Inputs may be any that keep to these rules, and one draw needn't show every extreme that they name: `route_ids`: in each aligned block of 16 positions, a row names 4 different experts and no expert is named by more than 4 rows; in every draw some expert reaches 4 in some block.
All inputs are finite; a program needn't handle non-finite values.
Results may differ from a plain program's by a relative error of at most 0.014.
Values may be sent and summed in bfloat16 or wider, within the bound.
A program may use at most 64 MiB of HBM per device.

v0:
```python
import jax
import jax.numpy as jnp
from jax import lax
from jax.sharding import PartitionSpec as P

clamp_limit = 7.0
sigmoid_scale = 1.702
epsilon = 1e-06


def passed_along(array, axis, by):
    count = lax.axis_size(axis)
    pairs = [(i, i + by) for i in range(count) if 0 <= i + by < count]
    return lax.ppermute(array, axis, pairs)


def clamped_units(gate_pre, up_pre):
    gate_cut = jnp.minimum(gate_pre, clamp_limit)
    up_cut = jnp.clip(up_pre, -clamp_limit, clamp_limit)
    return (up_cut + 1.0) * (gate_cut * jax.nn.sigmoid(sigmoid_scale * gate_cut))


def scaled_norm(values, gain):
    return (
        values
        * lax.rsqrt(jnp.mean(values * values, axis=-1, keepdims=True) + epsilon)
        * gain.astype(jnp.float32)
    )


def block_ranks(route_rows, experts, block_rows):
    flattened = route_rows.reshape(-1)
    entries = flattened.shape[0]
    span_width = block_rows * route_rows.shape[1]
    onehot = (flattened[:, None] == jnp.arange(experts, dtype=jnp.int32)[None, :]).astype(jnp.int32)
    blocked = onehot.reshape(entries // span_width, span_width, experts)
    before = jnp.cumsum(blocked, axis=1) - blocked
    return jnp.sum(before * blocked, axis=2).reshape(route_rows.shape)


def slot_picker(slot_index, table_size):
    matches = slot_index[None, :, :] == jnp.arange(table_size, dtype=jnp.int32)[:, None, None]
    return jnp.any(matches, axis=2).astype(jnp.bfloat16)


def local(
    stream_in,
    pre_gate,
    value_in,
    post_gate,
    conv_taps,
    out_weight,
    route_ids,
    route_weight,
    ffn_gain,
    post_gain,
    gate_proj,
    up_proj,
    down_proj,
):
    sp_count = lax.axis_size("sp")
    tp_count = lax.axis_size("tp")
    seq_rows = pre_gate.shape[0]
    own_rows = seq_rows // tp_count
    top_count = route_ids.shape[1]
    slots_each = 2 * own_rows * top_count // sp_count
    tap_count = conv_taps.shape[0]
    gated_input = (pre_gate.astype(jnp.float32) * value_in.astype(jnp.float32)).astype(jnp.bfloat16)
    rim_rows = passed_along(gated_input[seq_rows - tap_count + 1 :], "sp", 1)
    padded = jnp.concatenate([rim_rows, gated_input], 0).astype(jnp.float32)
    convolved = jnp.zeros(gated_input.shape, jnp.float32)
    for tap_index in range(tap_count):
        convolved = (
            convolved
            + conv_taps[tap_index].astype(jnp.float32)[None, :]
            * padded[tap_index : tap_index + seq_rows]
        )
    mixer_out = (post_gate.astype(jnp.float32) * convolved).astype(jnp.bfloat16)
    spread = lax.all_to_all(mixer_out, "tp", split_axis=0, concat_axis=1, tiled=True)
    projected = jnp.dot(
        spread,
        lax.all_gather(out_weight, "tp", axis=0, tiled=True),
        preferred_element_type=jnp.float32,
    )
    residual = (stream_in.astype(jnp.float32) + projected).astype(jnp.bfloat16)
    normed = scaled_norm(residual.astype(jnp.float32), ffn_gain).astype(jnp.bfloat16)
    slot_rank = block_ranks(route_ids, sp_count, own_rows)
    block_of = (jnp.arange(seq_rows, dtype=jnp.int32) // own_rows)[:, None]
    tp_index = lax.axis_index("tp")
    own_ids = lax.dynamic_slice_in_dim(route_ids, tp_index * own_rows, own_rows, 0)
    own_rank = lax.dynamic_slice_in_dim(slot_rank, tp_index * own_rows, own_rows, 0)
    own_slot = own_ids * slots_each + own_rank
    picker = slot_picker(own_slot, sp_count * slots_each)
    outgoing = jnp.dot(picker, normed, preferred_element_type=jnp.float32).astype(jnp.bfloat16)
    arrived = lax.all_to_all(outgoing, "sp", split_axis=0, concat_axis=0, tiled=True)
    portion = lax.all_gather(arrived, "tp", axis=0, tiled=True)
    gate_pre = jnp.dot(portion, gate_proj[0], preferred_element_type=jnp.float32)
    up_pre = jnp.dot(portion, up_proj[0], preferred_element_type=jnp.float32)
    hidden = clamped_units(gate_pre, up_pre).astype(jnp.bfloat16)
    weight_rows = down_proj[0]
    column_out = jnp.dot(
        lax.all_gather(hidden, "tp", axis=1, tiled=True),
        weight_rows,
        preferred_element_type=jnp.float32,
    ).astype(jnp.bfloat16)
    column_width = column_out.shape[1]
    returned = lax.all_to_all(
        column_out.reshape(tp_count, sp_count, slots_each, column_width),
        "sp",
        split_axis=1,
        concat_axis=1,
        tiled=True,
    )
    home_index = (block_of * sp_count + route_ids) * slots_each + slot_rank
    gathered_out = jnp.take(returned.reshape(-1, column_width), home_index.reshape(-1), axis=0)
    gathered_out = gathered_out.astype(jnp.float32).reshape(seq_rows, top_count, column_width)
    combined_cols = jnp.sum(gathered_out * route_weight[:, :, None], axis=1).astype(jnp.bfloat16)
    combined = lax.all_to_all(combined_cols, "tp", split_axis=0, concat_axis=1, tiled=True)
    layer_out = residual.astype(jnp.float32) + scaled_norm(combined.astype(jnp.float32), post_gain)
    return layer_out.astype(jnp.bfloat16)


def solution(mesh):
    placed = (
        P(("sp", "tp"), None),
        P("sp", "tp"),
        P("sp", "tp"),
        P("sp", "tp"),
        P(None, "tp"),
        P("tp", None),
        P("sp", None),
        P("sp", None),
        P(),
        P(),
        P("sp", None, "tp"),
        P("sp", None, "tp"),
        P("sp", None, "tp"),
    )
    return jax.shard_map(
        local, mesh=mesh, in_specs=placed, out_specs=P(("sp", "tp"), None), check_vma=False
    )
```

profile of v0, /device:TPU:1, one launch (start us, length us, event | category | flops | bytes accessed | tf_op | source)
XLA Modules:
  0.0 280.2 jit_solution(12051005114207174218)
XLA Ops:
  7.3 0.8 multiply_convert_fusion.2
  8.1 3.9 %collective-permute-start = (bf16[2,64]{0,1:T(8,128)(2,1)S(1)}, bf16[2,64]{0,1:T(8,128)(2,1)S(1)}, u32[]{:S(2)}, u32[]{:S(2)}) collective-permute-start(bf16[2,64]{0,1:T(8,128)(2,1)S(1)} %slice.30), channel_id=1, source_target_pairs={{0,16},{16,32},{32,48},{48,64},{64,80},{80,96},{96,112},{112,128},... | collective-permute-start | bytes 776 | tf_op jit(solution)/shard_map/ppermute | solution.py:14
  12.1 0.8 copy.62
  13.1 1.4 select_reduce_fusion
  14.7 0.8 bitcast_convert_fusion.2
  16.4 0.9 fusion.19
  18.1 8.1 %all-to-all-start = ((bf16[16,2,512]{2,1,0:T(2,128)(2,1)}), bf16[16,2,512]{2,1,0:T(2,128)(2,1)S(1)}, u32[]{:S(2)}, u32[]{:S(2)}) async-start(bf16[16,2,512]{2,1,0:T(2,128)(2,1)} %reshape.125), calls=%async_computation | async-start | bytes 65536 | tf_op jit(solution)/shard_map/all_to_all | solution.py:79
  26.3 7.3 %all-to-all-done = bf16[16,2,512]{2,1,0:T(2,128)(2,1)S(1)} async-done(((bf16[16,2,512]{2,1,0:T(2,128)(2,1)}), bf16[16,2,512]{2,1,0:T(2,128)(2,1)S(1)}, u32[]{:S(2)}, u32[]{:S(2)}) %all-to-all-start) | async-done | bytes 32800 | tf_op jit(solution)/shard_map/all_to_all | solution.py:79
  33.8 25.8 %all-gather.4.cloned.1.call-done = bf16[1024,2048]{1,0:T(8,128)(2,1)} async-done(((bf16[64,2048]{1,0:T(8,128)(2,1)}), bf16[1024,2048]{1,0:T(8,128)(2,1)}) %all-gather.4.cloned.1.call-update) | async-done | bytes 4194320 | tf_op jit(solution)/shard_map/all_gather | solution.py:82
  59.7 3.0 %multiply_reduce_fusion.1 = (f32[16]{0:T(128)S(1)}, f32[16,2048]{1,0:T(8,128)S(1)}) fusion(bf16[16,1024]{1,0:T(8,128)(2,1)S(1)} %all_to_all.36, bf16[1024,2048]{1,0:T(8,128)(2,1)} %all-gather.4.cloned.1.call-done, bf16[16,2048]{1,0:T(8,128)(2,1)} %param.13), kind=kOutput, calls=%fused_computation.29 | convolution fusion | flops 67305456 | bytes 4423744 | tf_op jit(solution)/shard_map/dot_general | solution.py:80
  63.2 26.7 %all_to_all.46 = bf16[32,4,2048]{2,1,0:T(4,128)(2,1)S(1)} all-to-all(bf16[32,4,2048]{2,1,0:T(4,128)(2,1)S(1)} %all_to_all.37), channel_id=1, replica_groups=mesh['sp'=32,'tp'=16] {'sp'}, dimensions={0} | all-to-all | bytes 1048576 | tf_op jit(solution)/shard_map/all_to_all | solution.py:95
  89.9 1.0 all_to_all.39
  90.9 53.9 %all-gather.6.cloned.1.call-done = bf16[2048,2048]{1,0:T(8,128)(2,1)} async-done(((bf16[128,2048]{1,0:T(8,128)(2,1)}), bf16[2048,2048]{1,0:T(8,128)(2,1)}) %all-gather.6.cloned.1.call-update) | async-done | bytes 8388624 | tf_op jit(solution)/shard_map/all_gather | solution.py:96
  144.8 5.9 %convolution_minimum_fusion = f32[2048,128]{1,0:T(8,128)S(1)} fusion(bf16[2048,2048]{1,0:T(8,128)(2,1)} %all-gather.6.cloned.1.call-done, bf16[1,2048,128]{2,1,0:T(8,128)(2,1)S(1)} %copy-done), kind=kOutput, calls=%fused_computation.1 | convolution fusion | flops 1074003968 | bytes 9961472 | tf_op jit(solution)/shard_map/dot_general | solution.py:97
  150.8 3.3 %fusion.2 = bf16[2048,128]{1,0:T(8,128)(2,1)} fusion(bf16[2048,2048]{1,0:T(8,128)(2,1)S(1)} %copy-done.4, f32[2048,128]{1,0:T(8,128)S(1)} %convolution_minimum_fusion, bf16[1,2048,128]{2,1,0:T(8,128)(2,1)S(1)} %copy-done.5), kind=kOutput, calls=%fused_computation.5 | convolution fusion | flops 1076101120 | bytes 10485760 | tf_op jit(solution)/shard_map/dot_general | solution.py:98
  154.1 68.6 %all-gather.8.cloned.1.call-done = bf16[2048,2048]{1,0:T(8,128)(2,1)} async-done(((bf16[2048,128]{1,0:T(8,128)(2,1)}), bf16[2048,2048]{1,0:T(8,128)(2,1)}) %all-gather.8.cloned.1.call-update) | async-done | bytes 8388624 | tf_op jit(solution)/shard_map/all_gather | solution.py:102
  222.8 5.7 %convolution_convert_fusion = bf16[2048,128]{1,0:T(8,128)(2,1)S(1)} fusion(bf16[2048,2048]{1,0:T(8,128)(2,1)} %all-gather.8.cloned.1.call-done, bf16[1,2048,128]{2,1,0:T(8,128)(2,1)S(1)} %copy-done.6), kind=kOutput, calls=%fused_computation.6 | convolution fusion | flops 1074003968 | bytes 9437184 | tf_op jit(solution)/shard_map/dot_general | solution.py:101
  228.5 1.1 copy.69
  229.6 6.9 %all-to-all-start.2 = ((bf16[16,32,4,128]{3,2,0,1:T(4,128)(2,1)}), bf16[16,32,4,128]{3,2,0,1:T(4,128)(2,1)S(1)}, u32[]{:S(2)}, u32[]{:S(2)}) async-start(bf16[16,32,4,128]{3,2,0,1:T(4,128)(2,1)} %copy.69), calls=%async_computation.2 | async-start | bytes 1048576 | tf_op jit(solution)/shard_map/all_to_all | solution.py:107
  237.2 15.9 %all-to-all-done.2 = bf16[16,32,4,128]{3,2,0,1:T(4,128)(2,1)S(1)} async-done(((bf16[16,32,4,128]{3,2,0,1:T(4,128)(2,1)}), bf16[16,32,4,128]{3,2,0,1:T(4,128)(2,1)S(1)}, u32[]{:S(2)}, u32[]{:S(2)}) %all-to-all-start.2) | async-done | bytes 524320 | tf_op jit(solution)/shard_map/all_to_all | solution.py:107
  253.3 3.2 %gather_fusion = bf16[1024,128]{1,0:T(8,128)(2,1)S(1)} fusion(bf16[2048,128]{1,0:T(8,128)(2,1)S(1)} %bitcast.43, s32[1024]{0:T(1024)S(1)} %broadcast_clamp_fusion), kind=kCustom, calls=%fused_computation | custom fusion | bytes 528384 | tf_op jit(solution)/shard_map/jit(_take)/gather | solution.py:115
  256.5 2.1 multiply_reduce_fusion
  258.6 6.4 %all-to-all-start.3 = ((bf16[16,16,128]{2,1,0:T(8,128)(2,1)}), bf16[16,16,128]{2,1,0:T(8,128)(2,1)S(1)}, u32[]{:S(2)}, u32[]{:S(2)}) async-start(bf16[16,16,128]{2,1,0:T(8,128)(2,1)} %bitcast.12), calls=%async_computation.3 | async-start | bytes 131072 | tf_op jit(solution)/shard_map/all_to_all | solution.py:118
  265.0 7.8 %all-to-all-done.3 = bf16[16,16,128]{2,1,0:T(8,128)(2,1)S(1)} async-done(((bf16[16,16,128]{2,1,0:T(8,128)(2,1)}), bf16[16,16,128]{2,1,0:T(8,128)(2,1)S(1)}, u32[]{:S(2)}, u32[]{:S(2)}) %all-to-all-start.3) | async-done | bytes 65568 | tf_op jit(solution)/shard_map/all_to_all | solution.py:118
  (53 shorter events, 5.7 us)
Async XLA Ops:
  6.5 138.3 %copy-start = (bf16[1,2048,128]{2,1,0:T(8,128)(2,1)S(1)}, bf16[1,2048,128]{2,1,0:T(8,128)(2,1)}, u32[]{:S(2)}) copy-start(bf16[1,2048,128]{2,1,0:T(8,128)(2,1)} %param.23) | copy-start | bytes 1572868
  6.5 53.1 %all-gather.4.cloned.1.call-start = ((), (), s32[]{:S(2)}) async-start(), calls=%async_computation.4 | async-start | bytes 4456448 | tf_op jit(solution)/shard_map/all_gather | solution.py:82
  8.1 8.2 %collective-permute-start = (bf16[2,64]{0,1:T(8,128)(2,1)S(1)}, bf16[2,64]{0,1:T(8,128)(2,1)S(1)}, u32[]{:S(2)}, u32[]{:S(2)}) collective-permute-start(bf16[2,64]{0,1:T(8,128)(2,1)S(1)} %slice.30), channel_id=1, source_target_pairs={{0,16},{16,32},{32,48},{48,64},{64,80},{80,96},{96,112},{112,128},... | collective-permute-start | bytes 776 | tf_op jit(solution)/shard_map/ppermute | solution.py:14
  18.1 15.5 %all-to-all-start = ((bf16[16,2,512]{2,1,0:T(2,128)(2,1)}), bf16[16,2,512]{2,1,0:T(2,128)(2,1)S(1)}, u32[]{:S(2)}, u32[]{:S(2)}) async-start(bf16[16,2,512]{2,1,0:T(2,128)(2,1)} %reshape.125), calls=%async_computation | async-start | bytes 65536 | tf_op jit(solution)/shard_map/all_to_all | solution.py:79
  26.2 118.6 %all-gather.6.cloned.1.call-start = ((), (), s32[]{:S(2)}) async-start(), calls=%async_computation.5 | async-start | bytes 8912896 | tf_op jit(solution)/shard_map/all_gather | solution.py:96
  62.6 88.1 %copy-start.5 = (bf16[1,2048,128]{2,1,0:T(8,128)(2,1)S(1)}, bf16[1,2048,128]{2,1,0:T(8,128)(2,1)}, u32[]{:S(2)}) copy-start(bf16[1,2048,128]{2,1,0:T(8,128)(2,1)} %param.24) | copy-start | bytes 1572868
  90.9 131.9 %all-gather.8.cloned.1.call-start = ((), (), s32[]{:S(2)}) async-start(), calls=%async_computation.6 | async-start | bytes 8912896 | tf_op jit(solution)/shard_map/all_gather | solution.py:102
  144.8 5.9 %copy-start.4 = (bf16[2048,2048]{1,0:T(8,128)(2,1)S(1)}, bf16[2048,2048]{1,0:T(8,128)(2,1)}, u32[]{:S(2)}) copy-start(bf16[2048,2048]{1,0:T(8,128)(2,1)} %all-gather.6.cloned.1.call-done) | copy-start | bytes 25165828
  150.8 72.0 %copy-start.6 = (bf16[1,2048,128]{2,1,0:T(8,128)(2,1)S(1)}, bf16[1,2048,128]{2,1,0:T(8,128)(2,1)}, u32[]{:S(2)}) copy-start(bf16[1,2048,128]{2,1,0:T(8,128)(2,1)} %param.25) | copy-start | bytes 1572868
  154.1 82.5 %copy-start.1 = (s32[256,4]{0,1:T(4,128)S(1)}, s32[256,4]{0,1:T(4,128)}, u32[]{:S(2)}) copy-start(s32[256,4]{0,1:T(4,128)} %param.19) | copy-start | bytes 12292
  154.1 83.0 %copy-start.2 = (f32[256,4]{0,1:T(4,128)S(1)}, f32[256,4]{0,1:T(4,128)}, u32[]{:S(2)}) copy-start(f32[256,4]{0,1:T(4,128)} %param.20) | copy-start | bytes 12292
  154.1 110.9 %copy-start.3 = (bf16[2048]{0:T(1024)(128)(2,1)S(1)}, bf16[2048]{0:T(1024)(128)(2,1)}, u32[]{:S(2)}) copy-start(bf16[2048]{0:T(1024)(128)(2,1)} %param.22) | copy-start | bytes 12292
  229.6 23.5 %all-to-all-start.2 = ((bf16[16,32,4,128]{3,2,0,1:T(4,128)(2,1)}), bf16[16,32,4,128]{3,2,0,1:T(4,128)(2,1)S(1)}, u32[]{:S(2)}, u32[]{:S(2)}) async-start(bf16[16,32,4,128]{3,2,0,1:T(4,128)(2,1)} %copy.69), calls=%async_computation.2 | async-start | bytes 1048576 | tf_op jit(solution)/shard_map/all_to_all | solution.py:107
  258.6 14.2 %all-to-all-start.3 = ((bf16[16,16,128]{2,1,0:T(8,128)(2,1)}), bf16[16,16,128]{2,1,0:T(8,128)(2,1)S(1)}, u32[]{:S(2)}, u32[]{:S(2)}) async-start(bf16[16,16,128]{2,1,0:T(8,128)(2,1)} %bitcast.12), calls=%async_computation.3 | async-start | bytes 131072 | tf_op jit(solution)/shard_map/all_to_all | solution.py:118
Sparse Core Ops, SparseCore 0:
  9.5 50.1 all-gather.3
  91.0 53.7 all-gather.5
  154.2 68.4 all-gather.7
where the time goes:
time: 281 us; the launch traced here: 280 us
  waiting for transfers between devices  180 us (64%)
  blocking collectives  26.7 us (10%)
  starting transfers between devices  25.4 us (9%)
  matrix products  18.2 us (6%)
  between operations  13.4 us (5%)
  local copies, waits for them, and re-layouts  8.78 us (3%)
  other arithmetic  7.76 us (3%)
    all_gather x1, waiting for transfers between devices, local(): lax.all_gather(hidden, 'tp', axis=1, tiled=True)  68.6 us
    all_gather x1, waiting for transfers between devices, local(): portion = lax.all_gather(arrived, 'tp', axis=0, tiled=True)  53.9 us
    all_to_all x1, blocking collectives, local(): lax.all_to_all(outgoing, 'sp', split_axis=0, concat_axis=0, tiled=True)  26.7 us
    all_gather x1, waiting for transfers between devices, local(): lax.all_gather(out_weight, 'tp', axis=0, tiled=True)  25.8 us
    all_to_all x1, waiting for transfers between devices, local(): lax.all_to_all(column_out.reshape(tp_count, sp_count, slots_each, column_...  15.9 us
    all_to_all x1, starting transfers between devices, local(): lax.all_to_all(mixer_out, 'tp', split_axis=0, concat_axis=1, tiled=True)  8.07 us
    all_to_all x1, waiting for transfers between devices, local(): lax.all_to_all(combined_cols, 'tp', split_axis=0, concat_axis=1, tiled=True)  7.76 us
    all_to_all x1, waiting for transfers between devices, local(): lax.all_to_all(mixer_out, 'tp', split_axis=0, concat_axis=1, tiled=True)  7.26 us
  transfers between devices with their start and end apart: 7, of which 6 were waited for; matrix products, arithmetic and copies ran while one was open for 3% of the time, Pallas kernels for 0%

commit v1 on v0

--- a/solution.py
+++ b/solution.py
@@ -93,7 +93,26 @@
     picker = slot_picker(own_slot, sp_count * slots_each)
     outgoing = jnp.dot(picker, normed, preferred_element_type=jnp.float32).astype(jnp.bfloat16)
     arrived = lax.all_to_all(outgoing, "sp", split_axis=0, concat_axis=0, tiled=True)
-    portion = lax.all_gather(arrived, "tp", axis=0, tiled=True)
+    length, index, extent = (lax.axis_size("tp"), lax.axis_index("tp"), arrived.shape[0])
+    upward = [(i_2, (i_2 + 1) % length) for i_2 in range(length)]
+    behind = [(i_2, (i_2 - 1) % length) for i_2 in range(length)]
+    result = jnp.zeros(
+        (*arrived.shape[:0], length * extent, *arrived.shape[0 + 1 :]), arrived.dtype
+    )
+    result = lax.dynamic_update_slice_in_dim(result, arrived, index * extent, axis=0)
+    from_left = from_right = arrived
+    half = length // 2
+    for step in range(1, half + 1):
+        from_left = lax.ppermute(from_left, "tp", upward)
+        result = lax.dynamic_update_slice_in_dim(
+            result, from_left, (index - step) % length * extent, axis=0
+        )
+        if step < length - half:
+            from_right = lax.ppermute(from_right, "tp", behind)
+            result = lax.dynamic_update_slice_in_dim(
+                result, from_right, (index + step) % length * extent, axis=0
+            )
+    portion = result
     gate_pre = jnp.dot(portion, gate_proj[0], preferred_element_type=jnp.float32)
     up_pre = jnp.dot(portion, up_proj[0], preferred_element_type=jnp.float32)
     hidden = clamped_units(gate_pre, up_pre).astype(jnp.bfloat16)

time: 281 us -> 298 us (1.060)
  starting transfers between devices: 25.4 us -> 60.1 us
  waiting for transfers between devices: 180 us -> 164 us
  matrix products: 18.2 us -> 14.8 us
    all_gather x1 -> x0, waiting for transfers between devices: 53.9 us -> none  [local(): portion = lax.all_gather(arrived, 'tp', axis=0, tiled=True)]
    ppermute x0 -> x15, waiting for transfers between devices: none -> 35.5 us  [the longest x8 27.9 us: local(): from_left = lax.ppermute(from_left, 'tp', upward)]
    ppermute x0 -> x15, starting transfers between devices: none -> 34.9 us  [the longest x8 19.5 us: local(): from_left = lax.ppermute(from_left, 'tp', upward)]
    dot_general x1, matrix products: 5.91 us -> 2.42 us  [local(): jnp.dot(portion, gate_proj[0], preferred_element_type=jnp.float32)]
  transfers between devices with their start and end apart: 7 -> 21, of which waited for: 6 -> 18; matrix products, arithmetic and copies ran while one was open for 3% -> 3% of each run, Pallas kernels for 0% -> 0%
where the time goes in v1:
time: 298 us; the launch traced here: 297 us
  waiting for transfers between devices  164 us (55%)
  starting transfers between devices  60.1 us (20%)
  blocking collectives  26.7 us (9%)
  matrix products  14.8 us (5%)
  between operations  13.8 us (5%)
  local copies, waits for them, and re-layouts  9.81 us (3%)
  other arithmetic  7.76 us (3%)
    all_gather x1, waiting for transfers between devices, local(): lax.all_gather(hidden, 'tp', axis=1, tiled=True)  71.4 us
    ppermute x8, waiting for transfers between devices, local(): from_left = lax.ppermute(from_left, 'tp', upward)  27.9 us
    all_to_all x1, blocking collectives, local(): lax.all_to_all(outgoing, 'sp', split_axis=0, concat_axis=0, tiled=True)  26.7 us
    all_gather x1, waiting for transfers between devices, local(): lax.all_gather(out_weight, 'tp', axis=0, tiled=True)  25.8 us
    ppermute x8, starting transfers between devices, local(): from_left = lax.ppermute(from_left, 'tp', upward)  19.5 us
    all_to_all x1, waiting for transfers between devices, local(): lax.all_to_all(column_out.reshape(tp_count, sp_count, slots_each, column_...  15.9 us
    ppermute x7, starting transfers between devices, local(): from_right = lax.ppermute(from_right, 'tp', behind)  15.3 us
    all_to_all x1, starting transfers between devices, local(): lax.all_to_all(mixer_out, 'tp', split_axis=0, concat_axis=1, tiled=True)  8.07 us
  transfers between devices with their start and end apart: 21, of which 18 were waited for; matrix products, arithmetic and copies ran while one was open for 3% of the time, Pallas kernels for 0%

profile of v1, /device:TPU:1, one launch (start us, length us, event | category | flops | bytes accessed | tf_op | source)
XLA Modules:
  0.0 297.4 jit_solution(2784480283935194933)
XLA Ops:
  8.1 3.9 %collective-permute-start = (bf16[2,64]{0,1:T(8,128)(2,1)S(1)}, bf16[2,64]{0,1:T(8,128)(2,1)S(1)}, u32[]{:S(2)}, u32[]{:S(2)}) collective-permute-start(bf16[2,64]{0,1:T(8,128)(2,1)S(1)} %slice.30), channel_id=1, source_target_pairs={{0,16},{16,32},{32,48},{48,64},{64,80},{80,96},{96,112},{112,128},... | collective-permute-start | bytes 776 | tf_op jit(solution)/shard_map/ppermute | solution.py:14
  18.1 8.1 %all-to-all-start = ((bf16[16,2,512]{2,1,0:T(2,128)(2,1)}), bf16[16,2,512]{2,1,0:T(2,128)(2,1)S(1)}, u32[]{:S(2)}, u32[]{:S(2)}) async-start(bf16[16,2,512]{2,1,0:T(2,128)(2,1)} %reshape.125), calls=%async_computation | async-start | bytes 65536 | tf_op jit(solution)/shard_map/all_to_all | solution.py:79
  26.3 7.3 %all-to-all-done = bf16[16,2,512]{2,1,0:T(2,128)(2,1)S(1)} async-done(((bf16[16,2,512]{2,1,0:T(2,128)(2,1)}), bf16[16,2,512]{2,1,0:T(2,128)(2,1)S(1)}, u32[]{:S(2)}, u32[]{:S(2)}) %all-to-all-start) | async-done | bytes 32800 | tf_op jit(solution)/shard_map/all_to_all | solution.py:79
  33.8 25.8 %all-gather.3.cloned.1.call-done = bf16[1024,2048]{1,0:T(8,128)(2,1)} async-done(((bf16[64,2048]{1,0:T(8,128)(2,1)}), bf16[1024,2048]{1,0:T(8,128)(2,1)}) %all-gather.3.cloned.1.call-update) | async-done | bytes 4194320 | tf_op jit(solution)/shard_map/all_gather | solution.py:82
  59.7 3.0 multiply_reduce_fusion.1
  63.2 26.7 %all_to_all.46 = bf16[32,4,2048]{2,1,0:T(4,128)(2,1)S(1)} all-to-all(bf16[32,4,2048]{2,1,0:T(4,128)(2,1)S(1)} %all_to_all.37), channel_id=1, replica_groups=mesh['sp'=32,'tp'=16] {'sp'}, dimensions={0} | all-to-all | bytes 1048576 | tf_op jit(solution)/shard_map/all_to_all | solution.py:95
  90.0 3.5 %collective-permute-start.1 = (bf16[128,2048]{1,0:T(8,128)(2,1)S(1)}, bf16[128,2048]{1,0:T(8,128)(2,1)S(1)}, u32[]{:S(2)}, u32[]{:S(2)}) collective-permute-start(bf16[128,2048]{1,0:T(8,128)(2,1)S(1)} %all_to_all.39), channel_id=1, source_target_pairs={{0,1},{1,2},{2,3},{3,4},{4,5},{5,6},{6,7},{7,8},{8,9},{9,10},{10,1... | collective-permute-start | bytes 1572872 | tf_op jit(solution)/shard_map/ppermute | solution.py:106
  93.5 6.1 %collective-permute-done.1 = bf16[128,2048]{1,0:T(8,128)(2,1)S(1)} collective-permute-done((bf16[128,2048]{1,0:T(8,128)(2,1)S(1)}, bf16[128,2048]{1,0:T(8,128)(2,1)S(1)}, u32[]{:S(2)}, u32[]{:S(2)}) %collective-permute-start.1) | collective-permute-done | bytes 524320 | tf_op jit(solution)/shard_map/ppermute | solution.py:106
  99.7 2.5 collective-permute-start.3
  102.2 6.1 %collective-permute-done.3 = bf16[128,2048]{1,0:T(8,128)(2,1)S(1)} collective-permute-done((bf16[128,2048]{1,0:T(8,128)(2,1)S(1)}, bf16[128,2048]{1,0:T(8,128)(2,1)S(1)}, u32[]{:S(2)}, u32[]{:S(2)}) %collective-permute-start.3) | collective-permute-done | bytes 524320 | tf_op jit(solution)/shard_map/ppermute | solution.py:106
  111.9 5.0 %collective-permute-done.5 = bf16[128,2048]{1,0:T(8,128)(2,1)S(1)} collective-permute-done((bf16[128,2048]{1,0:T(8,128)(2,1)S(1)}, bf16[128,2048]{1,0:T(8,128)(2,1)S(1)}, u32[]{:S(2)}, u32[]{:S(2)}) %collective-permute-start.5) | collective-permute-done | bytes 524320 | tf_op jit(solution)/shard_map/ppermute | solution.py:106
  123.0 2.5 collective-permute-done.7
  129.5 3.1 %collective-permute-start.10 = (bf16[128,2048]{1,0:T(8,128)(2,1)S(1)}, bf16[128,2048]{1,0:T(8,128)(2,1)S(1)}, u32[]{:S(2)}, u32[]{:S(2)}) collective-permute-start(bf16[128,2048]{1,0:T(8,128)(2,1)S(1)} %collective-permute-done.8), channel_id=1, source_target_pairs={{0,15},{1,0},{2,1},{3,2},{4,3},{5,4},{6,5},{7,6},{8,7},{9,8},{10,9... | collective-permute-start | bytes 1572872 | tf_op jit(solution)/shard_map/ppermute | solution.py:111
  138.4 4.0 %collective-permute-start.12 = (bf16[128,2048]{1,0:T(8,128)(2,1)S(1)}, bf16[128,2048]{1,0:T(8,128)(2,1)S(1)}, u32[]{:S(2)}, u32[]{:S(2)}) collective-permute-start(bf16[128,2048]{1,0:T(8,128)(2,1)S(1)} %collective-permute-done.10), channel_id=1, source_target_pairs={{0,15},{1,0},{2,1},{3,2},{4,3},{5,4},{6,5},{7,6},{8,7},{9,8},{10,9... | collective-permute-start | bytes 1572872 | tf_op jit(solution)/shard_map/ppermute | solution.py:111
  147.3 4.9 %collective-permute-start.14 = (bf16[128,2048]{1,0:T(8,128)(2,1)S(1)}, bf16[128,2048]{1,0:T(8,128)(2,1)S(1)}, u32[]{:S(2)}, u32[]{:S(2)}) collective-permute-start(bf16[128,2048]{1,0:T(8,128)(2,1)S(1)} %collective-permute-done.12), channel_id=1, source_target_pairs={{0,15},{1,0},{2,1},{3,2},{4,3},{5,4},{6,5},{7,6},{8,7},{9,8},{10,9... | collective-permute-start | bytes 1572872 | tf_op jit(solution)/shard_map/ppermute | solution.py:111
  156.2 6.1 %collective-permute-done.15 = bf16[128,2048]{1,0:T(8,128)(2,1)S(1)} collective-permute-done((bf16[128,2048]{1,0:T(8,128)(2,1)S(1)}, bf16[128,2048]{1,0:T(8,128)(2,1)S(1)}, u32[]{:S(2)}, u32[]{:S(2)}) %collective-permute-start.15) | collective-permute-done | bytes 524320 | tf_op jit(solution)/shard_map/ppermute | solution.py:106
  164.9 3.3 %fusion.2 = bf16[2048,128]{1,0:T(8,128)(2,1)} fusion(bf16[2048,2048]{1,0:T(8,128)(2,1)S(1)} %constant_dynamic-update-slice_fusion.15, f32[2048,128]{1,0:T(8,128)S(1)} %convolution_minimum_fusion, bf16[1,2048,128]{2,1,0:T(8,128)(2,1)S(1)} %copy-done.8), kind=kOutput, calls=%fused_computation.5 | convolution fusion | flops 1076101120 | bytes 10485760 | tf_op jit(solution)/shard_map/dot_general | solution.py:117
  168.3 71.4 %all-gather.5.cloned.1.call-done = bf16[2048,2048]{1,0:T(8,128)(2,1)} async-done(((bf16[2048,128]{1,0:T(8,128)(2,1)}), bf16[2048,2048]{1,0:T(8,128)(2,1)}) %all-gather.5.cloned.1.call-update) | async-done | bytes 8388624 | tf_op jit(solution)/shard_map/all_gather | solution.py:121
  239.7 5.7 %convolution_convert_fusion = bf16[2048,128]{1,0:T(8,128)(2,1)S(1)} fusion(bf16[2048,2048]{1,0:T(8,128)(2,1)} %all-gather.5.cloned.1.call-done, bf16[1,2048,128]{2,1,0:T(8,128)(2,1)S(1)} %copy-done.9), kind=kOutput, calls=%fused_computation.6 | convolution fusion | flops 1074003968 | bytes 9437184 | tf_op jit(solution)/shard_map/dot_general | solution.py:120
  246.6 6.8 %all-to-all-start.2 = ((bf16[16,32,4,128]{3,2,0,1:T(4,128)(2,1)}), bf16[16,32,4,128]{3,2,0,1:T(4,128)(2,1)S(1)}, u32[]{:S(2)}, u32[]{:S(2)}) async-start(bf16[16,32,4,128]{3,2,0,1:T(4,128)(2,1)} %copy.69), calls=%async_computation.2 | async-start | bytes 1048576 | tf_op jit(solution)/shard_map/all_to_all | solution.py:126
  254.1 15.9 %all-to-all-done.2 = bf16[16,32,4,128]{3,2,0,1:T(4,128)(2,1)S(1)} async-done(((bf16[16,32,4,128]{3,2,0,1:T(4,128)(2,1)}), bf16[16,32,4,128]{3,2,0,1:T(4,128)(2,1)S(1)}, u32[]{:S(2)}, u32[]{:S(2)}) %all-to-all-start.2) | async-done | bytes 524320 | tf_op jit(solution)/shard_map/all_to_all | solution.py:126
  270.3 3.2 %gather_fusion = bf16[1024,128]{1,0:T(8,128)(2,1)S(1)} fusion(bf16[2048,128]{1,0:T(8,128)(2,1)S(1)} %bitcast.43, s32[1024]{0:T(1024)S(1)} %broadcast_clamp_fusion), kind=kCustom, calls=%fused_computation | custom fusion | bytes 528384 | tf_op jit(solution)/shard_map/jit(_take)/gather | solution.py:134
  275.5 6.4 %all-to-all-start.3 = ((bf16[16,16,128]{2,1,0:T(8,128)(2,1)}), bf16[16,16,128]{2,1,0:T(8,128)(2,1)S(1)}, u32[]{:S(2)}, u32[]{:S(2)}) async-start(bf16[16,16,128]{2,1,0:T(8,128)(2,1)} %bitcast.12), calls=%async_computation.3 | async-start | bytes 131072 | tf_op jit(solution)/shard_map/all_to_all | solution.py:137
  282.0 7.8 %all-to-all-done.3 = bf16[16,16,128]{2,1,0:T(8,128)(2,1)S(1)} async-done(((bf16[16,16,128]{2,1,0:T(8,128)(2,1)}), bf16[16,16,128]{2,1,0:T(8,128)(2,1)S(1)}, u32[]{:S(2)}, u32[]{:S(2)}) %all-to-all-start.3) | async-done | bytes 65568 | tf_op jit(solution)/shard_map/all_to_all | solution.py:137
  (103 shorter events, 44.4 us)
Async XLA Ops:
  6.5 155.9 %copy-start = (bf16[1,2048,128]{2,1,0:T(8,128)(2,1)S(1)}, bf16[1,2048,128]{2,1,0:T(8,128)(2,1)}, u32[]{:S(2)}) copy-start(bf16[1,2048,128]{2,1,0:T(8,128)(2,1)} %param.23) | copy-start | bytes 1572868
  6.5 53.1 %all-gather.3.cloned.1.call-start = ((), (), s32[]{:S(2)}) async-start(), calls=%async_computation.4 | async-start | bytes 4456448 | tf_op jit(solution)/shard_map/all_gather | solution.py:82
  8.1 8.2 %collective-permute-start = (bf16[2,64]{0,1:T(8,128)(2,1)S(1)}, bf16[2,64]{0,1:T(8,128)(2,1)S(1)}, u32[]{:S(2)}, u32[]{:S(2)}) collective-permute-start(bf16[2,64]{0,1:T(8,128)(2,1)S(1)} %slice.30), channel_id=1, source_target_pairs={{0,16},{16,32},{32,48},{48,64},{64,80},{80,96},{96,112},{112,128},... | collective-permute-start | bytes 776 | tf_op jit(solution)/shard_map/ppermute | solution.py:14
  18.1 15.5 %all-to-all-start = ((bf16[16,2,512]{2,1,0:T(2,128)(2,1)}), bf16[16,2,512]{2,1,0:T(2,128)(2,1)S(1)}, u32[]{:S(2)}, u32[]{:S(2)}) async-start(bf16[16,2,512]{2,1,0:T(2,128)(2,1)} %reshape.125), calls=%async_computation | async-start | bytes 65536 | tf_op jit(solution)/shard_map/all_to_all | solution.py:79
  26.2 213.5 %all-gather.5.cloned.1.call-start = ((), (), s32[]{:S(2)}) async-start(), calls=%async_computation.5 | async-start | bytes 8912896 | tf_op jit(solution)/shard_map/all_gather | solution.py:121
  90.0 9.6 %collective-permute-start.1 = (bf16[128,2048]{1,0:T(8,128)(2,1)S(1)}, bf16[128,2048]{1,0:T(8,128)(2,1)S(1)}, u32[]{:S(2)}, u32[]{:S(2)}) collective-permute-start(bf16[128,2048]{1,0:T(8,128)(2,1)S(1)} %all_to_all.39), channel_id=1, source_target_pairs={{0,1},{1,2},{2,3},{3,4},{4,5},{5,6},{6,7},{7,8},{8,9},{9,10},{10,1... | collective-permute-start | bytes 1572872 | tf_op jit(solution)/shard_map/ppermute | solution.py:106
  93.5 8.6 %collective-permute-start.2 = (bf16[128,2048]{1,0:T(8,128)(2,1)S(1)}, bf16[128,2048]{1,0:T(8,128)(2,1)S(1)}, u32[]{:S(2)}, u32[]{:S(2)}) collective-permute-start(bf16[128,2048]{1,0:T(8,128)(2,1)S(1)} %all_to_all.39), channel_id=1, source_target_pairs={{0,15},{1,0},{2,1},{3,2},{4,3},{5,4},{6,5},{7,6},{8,7},{9,8},{10,9... | collective-permute-start | bytes 1572872 | tf_op jit(solution)/shard_map/ppermute | solution.py:111
  99.7 8.6 %collective-permute-start.3 = (bf16[128,2048]{1,0:T(8,128)(2,1)S(1)}, bf16[128,2048]{1,0:T(8,128)(2,1)S(1)}, u32[]{:S(2)}, u32[]{:S(2)}) collective-permute-start(bf16[128,2048]{1,0:T(8,128)(2,1)S(1)} %collective-permute-done.1), channel_id=1, source_target_pairs={{0,1},{1,2},{2,3},{3,4},{4,5},{5,6},{6,7},{7,8},{8,9},{9,10},{10,1... | collective-permute-start | bytes 1572872 | tf_op jit(solution)/shard_map/ppermute | solution.py:106
  102.2 8.9 %collective-permute-start.4 = (bf16[128,2048]{1,0:T(8,128)(2,1)S(1)}, bf16[128,2048]{1,0:T(8,128)(2,1)S(1)}, u32[]{:S(2)}, u32[]{:S(2)}) collective-permute-start(bf16[128,2048]{1,0:T(8,128)(2,1)S(1)} %collective-permute-done.2), channel_id=1, source_target_pairs={{0,15},{1,0},{2,1},{3,2},{4,3},{5,4},{6,5},{7,6},{8,7},{9,8},{10,9... | collective-permute-start | bytes 1572872 | tf_op jit(solution)/shard_map/ppermute | solution.py:111
  108.3 8.6 %collective-permute-start.5 = (bf16[128,2048]{1,0:T(8,128)(2,1)S(1)}, bf16[128,2048]{1,0:T(8,128)(2,1)S(1)}, u32[]{:S(2)}, u32[]{:S(2)}) collective-permute-start(bf16[128,2048]{1,0:T(8,128)(2,1)S(1)} %collective-permute-done.3), channel_id=1, source_target_pairs={{0,1},{1,2},{2,3},{3,4},{4,5},{5,6},{6,7},{7,8},{8,9},{9,10},{10,1... | collective-permute-start | bytes 1572872 | tf_op jit(solution)/shard_map/ppermute | solution.py:106
  111.1 9.5 %collective-permute-start.6 = (bf16[128,2048]{1,0:T(8,128)(2,1)S(1)}, bf16[128,2048]{1,0:T(8,128)(2,1)S(1)}, u32[]{:S(2)}, u32[]{:S(2)}) collective-permute-start(bf16[128,2048]{1,0:T(8,128)(2,1)S(1)} %collective-permute-done.4), channel_id=1, source_target_pairs={{0,15},{1,0},{2,1},{3,2},{4,3},{5,4},{6,5},{7,6},{8,7},{9,8},{10,9... | collective-permute-start | bytes 1572872 | tf_op jit(solution)/shard_map/ppermute | solution.py:111
  116.9 8.6 %collective-permute-start.7 = (bf16[128,2048]{1,0:T(8,128)(2,1)S(1)}, bf16[128,2048]{1,0:T(8,128)(2,1)S(1)}, u32[]{:S(2)}, u32[]{:S(2)}) collective-permute-start(bf16[128,2048]{1,0:T(8,128)(2,1)S(1)} %collective-permute-done.5), channel_id=1, source_target_pairs={{0,1},{1,2},{2,3},{3,4},{4,5},{5,6},{6,7},{7,8},{8,9},{9,10},{10,1... | collective-permute-start | bytes 1572872 | tf_op jit(solution)/shard_map/ppermute | solution.py:106
  120.6 8.9 %collective-permute-start.8 = (bf16[128,2048]{1,0:T(8,128)(2,1)S(1)}, bf16[128,2048]{1,0:T(8,128)(2,1)S(1)}, u32[]{:S(2)}, u32[]{:S(2)}) collective-permute-start(bf16[128,2048]{1,0:T(8,128)(2,1)S(1)} %collective-permute-done.6), channel_id=1, source_target_pairs={{0,15},{1,0},{2,1},{3,2},{4,3},{5,4},{6,5},{7,6},{8,7},{9,8},{10,9... | collective-permute-start | bytes 1572872 | tf_op jit(solution)/shard_map/ppermute | solution.py:111
  125.5 8.6 %collective-permute-start.9 = (bf16[128,2048]{1,0:T(8,128)(2,1)S(1)}, bf16[128,2048]{1,0:T(8,128)(2,1)S(1)}, u32[]{:S(2)}, u32[]{:S(2)}) collective-permute-start(bf16[128,2048]{1,0:T(8,128)(2,1)S(1)} %collective-permute-done.7), channel_id=1, source_target_pairs={{0,1},{1,2},{2,3},{3,4},{4,5},{5,6},{6,7},{7,8},{8,9},{9,10},{10,1... | collective-permute-start | bytes 1572872 | tf_op jit(solution)/shard_map/ppermute | solution.py:106
  129.5 8.9 %collective-permute-start.10 = (bf16[128,2048]{1,0:T(8,128)(2,1)S(1)}, bf16[128,2048]{1,0:T(8,128)(2,1)S(1)}, u32[]{:S(2)}, u32[]{:S(2)}) collective-permute-start(bf16[128,2048]{1,0:T(8,128)(2,1)S(1)} %collective-permute-done.8), channel_id=1, source_target_pairs={{0,15},{1,0},{2,1},{3,2},{4,3},{5,4},{6,5},{7,6},{8,7},{9,8},{10,9... | collective-permute-start | bytes 1572872 | tf_op jit(solution)/shard_map/ppermute | solution.py:111
  134.1 8.7 %collective-permute-start.11 = (bf16[128,2048]{1,0:T(8,128)(2,1)S(1)}, bf16[128,2048]{1,0:T(8,128)(2,1)S(1)}, u32[]{:S(2)}, u32[]{:S(2)}) collective-permute-start(bf16[128,2048]{1,0:T(8,128)(2,1)S(1)} %collective-permute-done.9), channel_id=1, source_target_pairs={{0,1},{1,2},{2,3},{3,4},{4,5},{5,6},{6,7},{7,8},{8,9},{9,10},{10,1... | collective-permute-start | bytes 1572872 | tf_op jit(solution)/shard_map/ppermute | solution.py:106
  138.4 8.9 %collective-permute-start.12 = (bf16[128,2048]{1,0:T(8,128)(2,1)S(1)}, bf16[128,2048]{1,0:T(8,128)(2,1)S(1)}, u32[]{:S(2)}, u32[]{:S(2)}) collective-permute-start(bf16[128,2048]{1,0:T(8,128)(2,1)S(1)} %collective-permute-done.10), channel_id=1, source_target_pairs={{0,15},{1,0},{2,1},{3,2},{4,3},{5,4},{6,5},{7,6},{8,7},{9,8},{10,9... | collective-permute-start | bytes 1572872 | tf_op jit(solution)/shard_map/ppermute | solution.py:111
  142.8 9.8 %collective-permute-start.13 = (bf16[128,2048]{1,0:T(8,128)(2,1)S(1)}, bf16[128,2048]{1,0:T(8,128)(2,1)S(1)}, u32[]{:S(2)}, u32[]{:S(2)}) collective-permute-start(bf16[128,2048]{1,0:T(8,128)(2,1)S(1)} %collective-permute-done.11), channel_id=1, source_target_pairs={{0,1},{1,2},{2,3},{3,4},{4,5},{5,6},{6,7},{7,8},{8,9},{9,10},{10,1... | collective-permute-start | bytes 1572872 | tf_op jit(solution)/shard_map/ppermute | solution.py:106
  147.3 8.9 %collective-permute-start.14 = (bf16[128,2048]{1,0:T(8,128)(2,1)S(1)}, bf16[128,2048]{1,0:T(8,128)(2,1)S(1)}, u32[]{:S(2)}, u32[]{:S(2)}) collective-permute-start(bf16[128,2048]{1,0:T(8,128)(2,1)S(1)} %collective-permute-done.12), channel_id=1, source_target_pairs={{0,15},{1,0},{2,1},{3,2},{4,3},{5,4},{6,5},{7,6},{8,7},{9,8},{10,9... | collective-permute-start | bytes 1572872 | tf_op jit(solution)/shard_map/ppermute | solution.py:111
  152.6 9.8 %collective-permute-start.15 = (bf16[128,2048]{1,0:T(8,128)(2,1)S(1)}, bf16[128,2048]{1,0:T(8,128)(2,1)S(1)}, u32[]{:S(2)}, u32[]{:S(2)}) collective-permute-start(bf16[128,2048]{1,0:T(8,128)(2,1)S(1)} %collective-permute-done.13), channel_id=1, source_target_pairs={{0,1},{1,2},{2,3},{3,4},{4,5},{5,6},{6,7},{7,8},{8,9},{9,10},{10,1... | collective-permute-start | bytes 1572872 | tf_op jit(solution)/shard_map/ppermute | solution.py:106
  168.3 85.7 %copy-start.6 = (f32[256,4]{0,1:T(4,128)S(1)}, f32[256,4]{0,1:T(4,128)}, u32[]{:S(2)}) copy-start(f32[256,4]{0,1:T(4,128)} %param.20) | copy-start | bytes 12292
  168.3 113.7 %copy-start.7 = (bf16[2048]{0:T(1024)(128)(2,1)S(1)}, bf16[2048]{0:T(1024)(128)(2,1)}, u32[]{:S(2)}) copy-start(bf16[2048]{0:T(1024)(128)(2,1)} %param.22) | copy-start | bytes 12292
  246.6 23.5 %all-to-all-start.2 = ((bf16[16,32,4,128]{3,2,0,1:T(4,128)(2,1)}), bf16[16,32,4,128]{3,2,0,1:T(4,128)(2,1)S(1)}, u32[]{:S(2)}, u32[]{:S(2)}) async-start(bf16[16,32,4,128]{3,2,0,1:T(4,128)(2,1)} %copy.69), calls=%async_computation.2 | async-start | bytes 1048576 | tf_op jit(solution)/shard_map/all_to_all | solution.py:126
  275.5 14.2 %all-to-all-start.3 = ((bf16[16,16,128]{2,1,0:T(8,128)(2,1)}), bf16[16,16,128]{2,1,0:T(8,128)(2,1)S(1)}, u32[]{:S(2)}, u32[]{:S(2)}) async-start(bf16[16,16,128]{2,1,0:T(8,128)(2,1)} %bitcast.12), calls=%async_computation.3 | async-start | bytes 131072 | tf_op jit(solution)/shard_map/all_to_all | solution.py:137
  (7 other events, 210.3 us)
Sparse Core Ops, SparseCore 0:
  9.5 50.1 all-gather.2
  168.4 71.2 all-gather.4
